TPU v7x, 32 devices: a whole 2x2x4 slice. The times are simulated.
32 devices in a mesh: fs: 8 (over z, y), tp: 4 (over x, core).
Axes of the slice: x: 2, y: 2, z: 4, core: 2. Of those that a mesh axis runs over, the one named last changes fastest.
Arguments:
- weights_in: float32 [2, 2048, 5632], P(None, 'fs', 'tp'), may hold values from -6 to 6
- weights_mix: float32 [2048, 2048], P('fs', 'tp'), may hold values from -6 to 6
- momentum_in: float32 [2, 2048, 5632], P(None, 'fs', 'tp'), may hold values from -5 to 5
- momentum_mix: float32 [2048, 2048], P('fs', 'tp'), may hold values from -5 to 5
- grads_in: float32 [2, 2048, 5632], P(None, 'fs', 'tp'), may hold values from -5 to 5
- grads_mix: float32 [2048, 2048], P('fs', 'tp'), may hold values from -5 to 5
Outputs:
- momentum_in_next: float32 [2, 2048, 5632], P(None, 'fs', 'tp')
- momentum_mix_next: float32 [2048, 2048], P('fs', 'tp')
- weights_in_next: float32 [2, 2048, 5632], P(None, 'fs', 'tp')
- weights_mix_next: float32 [2048, 2048], P('fs', 'tp')
- update_in: float32 [2, 2048, 5632], P(None, 'fs', 'tp')
- update_mix: float32 [2048, 2048], P('fs', 'tp')
All inputs are finite; a program needn't handle non-finite values.
Results may differ from a plain program's by a relative error of at most 0.0003.
Values sent between devices are 32-bit elements; how exact they have to be, the bound alone decides.
A program may use at most 128 MiB of HBM per device.

v0:
```python
import math
import jax
import jax.numpy as jnp
from jax import lax
from jax.sharding import PartitionSpec as P

D = 2048
FF = 5632
ITERS = 3
A_COEF = 3.4445
B_COEF = -4.775
C_COEF = 2.0315
MOMENTUM_DECAY = 0.95
STEP_RATE = 0.02
HIGH = lax.Precision.HIGHEST


def row_squares(shard):
    return jnp.sum(jnp.square(shard), axis=(1, 2))


def scale_from(summed):
    return (0.5 * lax.rsqrt(jnp.maximum(summed / D, 1.0)))[:, None, None]


def local(weights_in, weights_mix, momentum_in, momentum_mix, grads_in, grads_mix):
    moment_in = MOMENTUM_DECAY * momentum_in + grads_in
    moment_mix = MOMENTUM_DECAY * momentum_mix + grads_mix
    local_in = moment_in
    local_mix = moment_mix[None]
    squares = jnp.concatenate([row_squares(local_in), row_squares(local_mix)])
    scaling = scale_from(lax.psum(squares, ("fs", "tp")))
    for iteration in range(ITERS):
        cols_in, cols_mix = (
            lax.all_gather(local_in, "fs", axis=1, tiled=True),
            lax.all_gather(local_mix, "fs", axis=1, tiled=True),
        )
        partial_value = jnp.concatenate(
            [
                jnp.einsum("krc,ksc->krs", local_in, cols_in, precision=HIGH),
                jnp.einsum("krc,ksc->krs", local_mix, cols_mix, precision=HIGH),
            ]
        )
        gram_block = lax.psum_scatter(partial_value, "tp", scatter_dimension=2, tiled=True)
        gram_rows = lax.all_gather(gram_block, "tp", axis=2, tiled=True)
        factor = scaling if iteration == 0 else jnp.ones_like(scaling)
        gram_cols = lax.all_gather(gram_block, "fs", axis=1, tiled=True)
        square = jnp.einsum("krs,ksc->krc", gram_rows, gram_cols, precision=HIGH)
        poly_mat = factor**2 * B_COEF * gram_block + factor**4 * C_COEF * square
        poly_rows = lax.all_gather(poly_mat, "tp", axis=2, tiled=True)
        local_in = factor[:2] * (
            A_COEF * local_in + jnp.einsum("krs,ksc->krc", poly_rows[:2], cols_in, precision=HIGH)
        )
        local_mix = factor[2:] * (
            A_COEF * local_mix + jnp.einsum("krs,ksc->krc", poly_rows[2:], cols_mix, precision=HIGH)
        )
    step_in = local_in * math.sqrt(max(D, FF))
    step_mix = local_mix[0] * math.sqrt(D)
    return (
        moment_in,
        moment_mix,
        weights_in - STEP_RATE * step_in,
        weights_mix - STEP_RATE * step_mix,
        step_in,
        step_mix,
    )


def solution(mesh):
    in_specs = (
        P(None, "fs", "tp"),
        P("fs", "tp"),
        P(None, "fs", "tp"),
        P("fs", "tp"),
        P(None, "fs", "tp"),
        P("fs", "tp"),
    )
    out_specs = (
        P(None, "fs", "tp"),
        P("fs", "tp"),
        P(None, "fs", "tp"),
        P("fs", "tp"),
        P(None, "fs", "tp"),
        P("fs", "tp"),
    )
    return jax.shard_map(local, mesh=mesh, in_specs=in_specs, out_specs=out_specs, check_vma=False)
```

profile of v0, /device:TPU:0, one launch (start us, length us, event | category | flops | bytes accessed | tf_op | source)
XLA Modules:
  0.0 2754.7 jit_solution(12206210918786785973)
XLA Ops:
  14.7 71.5 %all-gather.43.cloned.1.call-done = f32[2048,512]{1,0:T(8,128)} async-done(((f32[256,512]{1,0:T(8,128)}), f32[2048,512]{1,0:T(8,128)}) %all-gather.43.cloned.1.call-update) | async-done | bytes 4194320 | tf_op jit(solution)/shard_map/all_gather | solution.py:36
  93.4 434.6 %all-gather.19.cloned.1.call-done = f32[2,2048,1408]{2,1,0:T(8,128)} async-done(((f32[2,256,1408]{2,1,0:T(8,128)}), f32[2,2048,1408]{2,1,0:T(8,128)}) %all-gather.19.cloned.1.call-update) | async-done | bytes 23068688 | tf_op jit(solution)/shard_map/all_gather | solution.py:35
  528.0 24.5 fusion.8
  555.7 58.0 %reduce-scatter.4.cloned.1.call-done = f32[3,256,512]{2,1,0:T(8,128)} async-done(((f32[3,256,2048]{2,1,0:T(8,128)}), f32[3,256,512]{2,1,0:T(8,128)}) %reduce-scatter.4.cloned.1.call-update) | async-done | bytes 1572880 | tf_op jit(solution)/shard_map/reduce_scatter | solution.py:44
  615.0 40.5 %psum.7 = f32[3]{0:T(128)S(1)} all-reduce(f32[3]{0:T(128)S(1)} %pad_maximum_fusion.3), channel_id=1, replica_groups=mesh['fs'=8,'tp'=4] {'fs','tp'}, use_global_device_ids=true, to_apply=%region_2.0 | all-reduce | flops 3 | bytes 24 | tf_op jit(solution)/shard_map/psum | solution.py:32
  662.3 178.2 %all-gather.23.cloned.1.call-done = f32[3,2048,512]{2,1,0:T(8,128)} async-done(((f32[3,256,512]{2,1,0:T(8,128)}), f32[3,2048,512]{2,1,0:T(8,128)}) %all-gather.23.cloned.1.call-update) | async-done | bytes 12582928 | tf_op jit(solution)/shard_map/all_gather | solution.py:47
  858.7 44.1 %all-gather.25.cloned.1.call-done = f32[3,256,2048]{2,1,0:T(8,128)} async-done(((f32[3,256,512]{2,1,0:T(8,128)}), f32[3,256,2048]{2,1,0:T(8,128)}) %all-gather.25.cloned.1.call-update) | async-done | bytes 6291472 | tf_op jit(solution)/shard_map/all_gather | solution.py:50
  911.3 27.5 fusion
  939.0 44.6 %all-gather.45.cloned.1.call-done = f32[2048,512]{1,0:T(8,128)} async-done(((f32[256,512]{1,0:T(8,128)}), f32[2048,512]{1,0:T(8,128)}) %all-gather.45.cloned.1.call-update) | async-done | bytes 4194320 | tf_op jit(solution)/shard_map/all_gather | solution.py:36
  990.8 434.6 %all-gather.27.cloned.1.call-done = f32[2,2048,1408]{2,1,0:T(8,128)} async-done(((f32[2,256,1408]{2,1,0:T(8,128)}), f32[2,2048,1408]{2,1,0:T(8,128)}) %all-gather.27.cloned.1.call-update) | async-done | bytes 23068688 | tf_op jit(solution)/shard_map/all_gather | solution.py:35
  1425.4 24.5 fusion.9
  1453.1 58.0 %reduce-scatter.6.cloned.1.call-done = f32[3,256,512]{2,1,0:T(8,128)} async-done(((f32[3,256,2048]{2,1,0:T(8,128)}), f32[3,256,512]{2,1,0:T(8,128)}) %reduce-scatter.6.cloned.1.call-update) | async-done | bytes 1572880 | tf_op jit(solution)/shard_map/reduce_scatter | solution.py:44
  1512.1 46.8 %all-gather.29.cloned.1.call-done = f32[3,256,2048]{2,1,0:T(8,128)} async-done(((f32[3,256,512]{2,1,0:T(8,128)}), f32[3,256,2048]{2,1,0:T(8,128)}) %all-gather.29.cloned.1.call-update) | async-done | bytes 6291472 | tf_op jit(solution)/shard_map/all_gather | solution.py:45
  1558.9 178.3 %all-gather.31.cloned.1.call-done = f32[3,2048,512]{2,1,0:T(8,128)} async-done(((f32[3,256,512]{2,1,0:T(8,128)}), f32[3,2048,512]{2,1,0:T(8,128)}) %all-gather.31.cloned.1.call-update) | async-done | bytes 12582928 | tf_op jit(solution)/shard_map/all_gather | solution.py:47
  1754.8 44.6 %all-gather.33.cloned.1.call-done = f32[3,256,2048]{2,1,0:T(8,128)} async-done(((f32[3,256,512]{2,1,0:T(8,128)}), f32[3,256,2048]{2,1,0:T(8,128)}) %all-gather.33.cloned.1.call-update) | async-done | bytes 6291472 | tf_op jit(solution)/shard_map/all_gather | solution.py:50
  1807.1 27.4 convolution_add_fusion.1
  1835.0 44.7 %all-gather.47.cloned.1.call-done = f32[2048,512]{1,0:T(8,128)} async-done(((f32[256,512]{1,0:T(8,128)}), f32[2048,512]{1,0:T(8,128)}) %all-gather.47.cloned.1.call-update) | async-done | bytes 4194320 | tf_op jit(solution)/shard_map/all_gather | solution.py:36
  1886.9 434.4 %all-gather.35.cloned.1.call-done = f32[2,2048,1408]{2,1,0:T(8,128)} async-done(((f32[2,256,1408]{2,1,0:T(8,128)}), f32[2,2048,1408]{2,1,0:T(8,128)}) %all-gather.35.cloned.1.call-update) | async-done | bytes 23068688 | tf_op jit(solution)/shard_map/all_gather | solution.py:35
  2321.3 24.5 fusion.10
  2349.1 58.0 %reduce-scatter.8.cloned.1.call-done = f32[3,256,512]{2,1,0:T(8,128)} async-done(((f32[3,256,2048]{2,1,0:T(8,128)}), f32[3,256,512]{2,1,0:T(8,128)}) %reduce-scatter.8.cloned.1.call-update) | async-done | bytes 1572880 | tf_op jit(solution)/shard_map/reduce_scatter | solution.py:44
  2407.9 47.0 %all-gather.37.cloned.1.call-done = f32[3,256,2048]{2,1,0:T(8,128)} async-done(((f32[3,256,512]{2,1,0:T(8,128)}), f32[3,256,2048]{2,1,0:T(8,128)}) %all-gather.37.cloned.1.call-update) | async-done | bytes 6291472 | tf_op jit(solution)/shard_map/all_gather | solution.py:45
  2454.8 178.2 %all-gather.39.cloned.1.call-done = f32[3,2048,512]{2,1,0:T(8,128)} async-done(((f32[3,256,512]{2,1,0:T(8,128)}), f32[3,2048,512]{2,1,0:T(8,128)}) %all-gather.39.cloned.1.call-update) | async-done | bytes 12582928 | tf_op jit(solution)/shard_map/all_gather | solution.py:47
  2650.5 44.7 %all-gather.41.cloned.1.call-done = f32[3,256,2048]{2,1,0:T(8,128)} async-done(((f32[3,256,512]{2,1,0:T(8,128)}), f32[3,256,2048]{2,1,0:T(8,128)}) %all-gather.41.cloned.1.call-update) | async-done | bytes 6291472 | tf_op jit(solution)/shard_map/all_gather | solution.py:50
  2695.2 46.1 %broadcast_multiply_fusion = (f32[2,256,1408]{2,1,0:T(8,128)}, f32[2,256,1408]{2,1,0:T(8,128)}) fusion(f32[2,256,1408]{2,1,0:T(8,128)} %param.6, f32[3,256,2048]{2,1,0:T(8,128)} %all-gather.41.cloned.1.call-done, f32[2,2048,1408]{2,1,0:T(8,128)} %all-gather.35.cloned.1.call-done, f32[2,256,1408]{2,1,0:T(8,128)S(1)} %copy-done.2), kind=kOutput, calls=%fused_computation.22 | convolution fusion | flops 17720344576 | bytes 40894464 | tf_op jit(solution)/shard_map/krs,ksc->krc/dot_general | solution.py:52
  (77 shorter events, 124.9 us)
Async XLA Ops:
  7.2 79.1 %all-gather.43.cloned.1.call-start = ((), (), s32[]{:S(2)}) async-start(), calls=%async_computation.18 | async-start | bytes 4718592 | tf_op jit(solution)/shard_map/all_gather | solution.py:36
  9.9 76.3 %copy-start.9 = (f32[256,512]{1,0:T(8,128)S(1)}, f32[256,512]{1,0:T(8,128)}, u32[]{:S(2)}) copy-start(f32[256,512]{1,0:T(8,128)} %get-tuple-element.11) | copy-start | bytes 1572868
  9.9 518.0 %all-gather.19.cloned.1.call-start = ((), (), s32[]{:S(2)}) async-start(), calls=%async_computation.3 | async-start | bytes 25952256 | tf_op jit(solution)/shard_map/all_gather | solution.py:35
  14.7 513.3 %copy-start = (f32[2,256,1408]{2,1,0:T(8,128)S(1)}, f32[2,256,1408]{2,1,0:T(8,128)}, u32[]{:S(2)}) copy-start(f32[2,256,1408]{2,1,0:T(8,128)} %get-tuple-element.9) | copy-start | bytes 8650756
  14.7 599.0 %reduce-scatter.4.cloned.1.call-start = ((), (), s32[]{:S(2)}) async-start(), calls=%async_computation.4 | async-start | bytes 7864320 | tf_op jit(solution)/shard_map/reduce_scatter | solution.py:44
  555.6 106.7 %all-gather.21.cloned.1.call-start = ((), (), s32[]{:S(2)}) async-start(), calls=%async_computation.5 | async-start | bytes 7864320 | tf_op jit(solution)/shard_map/all_gather | solution.py:45
  613.7 226.8 %all-gather.23.cloned.1.call-start = ((), (), s32[]{:S(2)}) async-start(), calls=%async_computation.6 | async-start | bytes 14155776 | tf_op jit(solution)/shard_map/all_gather | solution.py:47
  614.3 288.5 %all-gather.25.cloned.1.call-start = ((), (), s32[]{:S(2)}) async-start(), calls=%async_computation.7 | async-start | bytes 7864320 | tf_op jit(solution)/shard_map/all_gather | solution.py:50
  858.0 125.6 %all-gather.45.cloned.1.call-start = ((), (), s32[]{:S(2)}) async-start(), calls=%async_computation.19 | async-start | bytes 4718592 | tf_op jit(solution)/shard_map/all_gather | solution.py:36
  910.7 514.7 %all-gather.27.cloned.1.call-start = ((), (), s32[]{:S(2)}) async-start(), calls=%async_computation.8 | async-start | bytes 25952256 | tf_op jit(solution)/shard_map/all_gather | solution.py:35
  911.3 72.4 %copy-start.5 = (f32[256,512]{1,0:T(8,128)S(1)}, f32[256,512]{1,0:T(8,128)}, u32[]{:S(2)}) copy-start(f32[256,512]{1,0:T(8,128)} %fusion.5) | copy-start | bytes 1572868
  938.8 486.6 %copy-start.1 = (f32[2,256,1408]{2,1,0:T(8,128)S(1)}, f32[2,256,1408]{2,1,0:T(8,128)}, u32[]{:S(2)}) copy-start(f32[2,256,1408]{2,1,0:T(8,128)} %fusion) | copy-start | bytes 8650756
  938.8 572.3 %reduce-scatter.6.cloned.1.call-start = ((), (), s32[]{:S(2)}) async-start(), calls=%async_computation.9 | async-start | bytes 7864320 | tf_op jit(solution)/shard_map/reduce_scatter | solution.py:44
  1453.1 105.8 %all-gather.29.cloned.1.call-start = ((), (), s32[]{:S(2)}) async-start(), calls=%async_computation.10 | async-start | bytes 7864320 | tf_op jit(solution)/shard_map/all_gather | solution.py:45
  1511.1 226.1 %all-gather.31.cloned.1.call-start = ((), (), s32[]{:S(2)}) async-start(), calls=%async_computation.11 | async-start | bytes 14155776 | tf_op jit(solution)/shard_map/all_gather | solution.py:47
  1511.9 287.6 %all-gather.33.cloned.1.call-start = ((), (), s32[]{:S(2)}) async-start(), calls=%async_computation.12 | async-start | bytes 7864320 | tf_op jit(solution)/shard_map/all_gather | solution.py:50
  1754.8 125.0 %all-gather.47.cloned.1.call-start = ((), (), s32[]{:S(2)}) async-start(), calls=%async_computation.20 | async-start | bytes 4718592 | tf_op jit(solution)/shard_map/all_gather | solution.py:36
  1806.8 73.0 %copy-start.4 = (f32[256,512]{1,0:T(8,128)S(1)}, f32[256,512]{1,0:T(8,128)}, u32[]{:S(2)}) copy-start(f32[256,512]{1,0:T(8,128)} %fusion.6) | copy-start | bytes 1572868
  1806.8 514.5 %all-gather.35.cloned.1.call-start = ((), (), s32[]{:S(2)}) async-start(), calls=%async_computation.13 | async-start | bytes 25952256 | tf_op jit(solution)/shard_map/all_gather | solution.py:35
  1834.5 486.8 %copy-start.2 = (f32[2,256,1408]{2,1,0:T(8,128)S(1)}, f32[2,256,1408]{2,1,0:T(8,128)}, u32[]{:S(2)}) copy-start(f32[2,256,1408]{2,1,0:T(8,128)} %convolution_add_fusion.1) | copy-start | bytes 8650756
  1834.5 572.5 %reduce-scatter.8.cloned.1.call-start = ((), (), s32[]{:S(2)}) async-start(), calls=%async_computation.14 | async-start | bytes 7864320 | tf_op jit(solution)/shard_map/reduce_scatter | solution.py:44
  2349.0 105.8 %all-gather.37.cloned.1.call-start = ((), (), s32[]{:S(2)}) async-start(), calls=%async_computation.15 | async-start | bytes 7864320 | tf_op jit(solution)/shard_map/all_gather | solution.py:45
  2407.0 225.9 %all-gather.39.cloned.1.call-start = ((), (), s32[]{:S(2)}) async-start(), calls=%async_computation.16 | async-start | bytes 14155776 | tf_op jit(solution)/shard_map/all_gather | solution.py:47
  2407.6 287.6 %all-gather.41.cloned.1.call-start = ((), (), s32[]{:S(2)}) async-start(), calls=%async_computation.17 | async-start | bytes 7864320 | tf_op jit(solution)/shard_map/all_gather | solution.py:50
  (5 other events, 165.8 us)
Sparse Core Ops, SparseCore 0:
  10.7 75.5 all-gather.42
  88.3 439.5 all-gather.18
  555.8 57.8 reduce-scatter.3
  615.1 47.2 all-gather.20
  664.4 176.0 all-gather.22
  858.2 44.5 all-gather.24
  910.8 72.7 all-gather.44
  985.8 439.5 all-gather.26
  1453.2 57.8 reduce-scatter.5
  1512.5 46.3 all-gather.28
  1561.1 176.0 all-gather.30
  1754.9 44.5 all-gather.32
  1806.9 72.7 all-gather.46
  1881.7 439.5 all-gather.34
  2349.1 57.8 reduce-scatter.7
  2408.4 46.3 all-gather.36
  2456.8 176.0 all-gather.38
  2650.7 44.5 all-gather.40
where the time goes:
time: 2760 us; the launch traced here: 2750 us
  waiting for transfers between devices  2410 us (87%)
  matrix products  270 us (10%)
  blocking collectives  40.5 us (1%)
    all_gather x3, waiting for transfers between devices, local(): lax.all_gather(local_in, 'fs', axis=1, tiled=True)  1300 us
    all_gather x3, waiting for transfers between devices, local(): gram_cols = lax.all_gather(gram_block, 'fs', axis=1, tiled=True)  535 us
    reduce_scatter x3, waiting for transfers between devices, local(): lax.psum_scatter(partial_value, 'tp', scatter_dimension=2, tiled=True)  174 us
    all_gather x3, waiting for transfers between devices, local(): lax.all_gather(local_mix, 'fs', axis=1, tiled=True)  161 us
    all_gather x3, waiting for transfers between devices, local(): poly_rows = lax.all_gather(poly_mat, 'tp', axis=2, tiled=True)  133 us
    dot_general x3, matrix products, local(): jnp.einsum('krs,ksc->krc', poly_rows[:2], cols_in, precision=HIGH)  101 us
    all_gather x3, waiting for transfers between devices, local(): gram_rows = lax.all_gather(gram_block, 'tp', axis=2, tiled=True)  100 us
    dot_general x3, matrix products, local(): jnp.einsum('krc,ksc->krs', local_in, cols_in, precision=HIGH)  73.6 us
  transfers between devices with their start and end apart: 18, of which 18 were waited for; matrix products, arithmetic and copies ran while one was open for 3% of the time, Pallas kernels for 0%

commit v1 on v0

--- a/solution.py
+++ b/solution.py
@@ -32,7 +32,9 @@
     scaling = scale_from(lax.psum(squares, ("fs", "tp")))
     for iteration in range(ITERS):
         cols_in, cols_mix = (
-            lax.all_gather(local_in, "fs", axis=1, tiled=True),
+            jnp.concatenate(
+                lax.all_to_all(jnp.stack(lax.axis_size("fs") * [local_in]), "fs", 0, 0), axis=1
+            ),
             lax.all_gather(local_mix, "fs", axis=1, tiled=True),
         )
         partial_value = jnp.concatenate(

time: 2760 us -> 2980 us (1.080)
  waiting for transfers between devices: 2410 us -> 2550 us
  local copies, waits for them, and re-layouts: 0.63 us -> 58.7 us
    all_gather x3 -> x0, waiting for transfers between devices: 1300 us -> none  [local(): lax.all_gather(local_in, 'fs', axis=1, tiled=True)]
    all_gather x3, waiting for transfers between devices: 161 us -> 1310 us  [local(): lax.all_gather(local_mix, 'fs', axis=1, tiled=True)]
    all_to_all x0 -> x3, waiting for transfers between devices: none -> 293 us  [local(): lax.all_to_all(jnp.stack(lax.axis_size('fs') * [local_in]), 'fs', 0, 0)]
    another operation x0 -> x3, local copies, waits for them, and re-layouts: none -> 31.4 us  [local(): jnp.stack(lax.axis_size('fs') * [local_in])]
  transfers between devices with their start and end apart: 18 -> 18, of which waited for: 18 -> 18; matrix products, arithmetic and copies ran while one was open for 3% -> 1% of each run, Pallas kernels for 0% -> 0%
where the time goes in v1:
time: 2980 us; the launch traced here: 2970 us
  waiting for transfers between devices  2550 us (86%)
  matrix products  267 us (9%)
  local copies, waits for them, and re-layouts  58.7 us (2%)
  blocking collectives  40.4 us (1%)
    all_gather x3, waiting for transfers between devices, local(): lax.all_gather(local_mix, 'fs', axis=1, tiled=True)  1310 us
    all_gather x3, waiting for transfers between devices, local(): gram_cols = lax.all_gather(gram_block, 'fs', axis=1, tiled=True)  535 us
    all_to_all x3, waiting for transfers between devices, local(): lax.all_to_all(jnp.stack(lax.axis_size('fs') * [local_in]), 'fs', 0, 0)  293 us
    reduce_scatter x3, waiting for transfers between devices, local(): lax.psum_scatter(partial_value, 'tp', scatter_dimension=2, tiled=True)  169 us
    all_gather x3, waiting for transfers between devices, local(): poly_rows = lax.all_gather(poly_mat, 'tp', axis=2, tiled=True)  134 us
    all_gather x3, waiting for transfers between devices, local(): gram_rows = lax.all_gather(gram_block, 'tp', axis=2, tiled=True)  101 us
    dot_general x3, matrix products, local(): jnp.einsum('krs,ksc->krc', poly_rows[:2], cols_in, precision=HIGH)  101 us
    dot_general x3, matrix products, local(): jnp.einsum('krc,ksc->krs', local_in, cols_in, precision=HIGH)  71.3 us
  transfers between devices with their start and end apart: 18, of which 18 were waited for; matrix products, arithmetic and copies ran while one was open for 1% of the time, Pallas kernels for 0%

profile of v1, /device:TPU:0, one launch (start us, length us, event | category | flops | bytes accessed | tf_op | source)
XLA Modules:
  0.0 2970.1 jit_solution(11591520641135120827)
XLA Ops:
  30.3 441.2 %all-gather.34.cloned.1.call-done = f32[2048,512]{1,0:T(8,128)} async-done(((f32[256,512]{1,0:T(8,128)}), f32[2048,512]{1,0:T(8,128)}) %all-gather.34.cloned.1.call-update) | async-done | bytes 4194320 | tf_op jit(solution)/shard_map/all_gather | solution.py:38
  478.8 97.7 %all-to-all-done = f32[8,2,256,1408]{3,2,1,0:T(8,128)} async-done(((f32[8,2,256,1408]{3,2,1,0:T(8,128)}), f32[8,2,256,1408]{3,2,1,0:T(8,128)}, u32[]{:S(2)}, u32[]{:S(2)}) %all-to-all-start) | async-done | bytes 23068704 | tf_op jit(solution)/shard_map/all_to_all | solution.py:36
  585.6 22.5 fusion.8
  613.7 57.0 %reduce-scatter.4.cloned.1.call-done = f32[3,256,512]{2,1,0:T(8,128)} async-done(((f32[3,256,2048]{2,1,0:T(8,128)}), f32[3,256,512]{2,1,0:T(8,128)}) %reduce-scatter.4.cloned.1.call-update) | async-done | bytes 1572880 | tf_op jit(solution)/shard_map/reduce_scatter | solution.py:46
  672.1 40.4 %psum.7 = f32[3]{0:T(128)S(1)} all-reduce(f32[3]{0:T(128)S(1)} %pad_maximum_fusion.3), channel_id=1, replica_groups=mesh['fs'=8,'tp'=4] {'fs','tp'}, use_global_device_ids=true, to_apply=%region_2.0 | all-reduce | flops 3 | bytes 24 | tf_op jit(solution)/shard_map/psum | solution.py:32
  719.6 178.2 %all-gather.18.cloned.1.call-done = f32[3,2048,512]{2,1,0:T(8,128)} async-done(((f32[3,256,512]{2,1,0:T(8,128)}), f32[3,2048,512]{2,1,0:T(8,128)}) %all-gather.18.cloned.1.call-update) | async-done | bytes 12582928 | tf_op jit(solution)/shard_map/all_gather | solution.py:49
  915.2 44.7 %all-gather.20.cloned.1.call-done = f32[3,256,2048]{2,1,0:T(8,128)} async-done(((f32[3,256,512]{2,1,0:T(8,128)}), f32[3,256,2048]{2,1,0:T(8,128)}) %all-gather.20.cloned.1.call-update) | async-done | bytes 6291472 | tf_op jit(solution)/shard_map/all_gather | solution.py:52
  959.9 27.8 fusion
  1014.6 435.0 %all-gather.36.cloned.1.call-done = f32[2048,512]{1,0:T(8,128)} async-done(((f32[256,512]{1,0:T(8,128)}), f32[2048,512]{1,0:T(8,128)}) %all-gather.36.cloned.1.call-update) | async-done | bytes 4194320 | tf_op jit(solution)/shard_map/all_gather | solution.py:38
  1456.9 97.8 %all-to-all-done.1 = f32[8,2,256,1408]{3,2,1,0:T(8,128)} async-done(((f32[8,2,256,1408]{3,2,1,0:T(8,128)}), f32[8,2,256,1408]{3,2,1,0:T(8,128)}, u32[]{:S(2)}, u32[]{:S(2)}) %all-to-all-start.1) | async-done | bytes 23068704 | tf_op jit(solution)/shard_map/all_to_all | solution.py:36
  1563.5 24.4 fusion.9
  1592.8 56.1 %reduce-scatter.6.cloned.1.call-done = f32[3,256,512]{2,1,0:T(8,128)} async-done(((f32[3,256,2048]{2,1,0:T(8,128)}), f32[3,256,512]{2,1,0:T(8,128)}) %reduce-scatter.6.cloned.1.call-update) | async-done | bytes 1572880 | tf_op jit(solution)/shard_map/reduce_scatter | solution.py:46
  1650.1 46.7 %all-gather.22.cloned.1.call-done = f32[3,256,2048]{2,1,0:T(8,128)} async-done(((f32[3,256,512]{2,1,0:T(8,128)}), f32[3,256,2048]{2,1,0:T(8,128)}) %all-gather.22.cloned.1.call-update) | async-done | bytes 6291472 | tf_op jit(solution)/shard_map/all_gather | solution.py:47
  1696.9 178.3 %all-gather.24.cloned.1.call-done = f32[3,2048,512]{2,1,0:T(8,128)} async-done(((f32[3,256,512]{2,1,0:T(8,128)}), f32[3,2048,512]{2,1,0:T(8,128)}) %all-gather.24.cloned.1.call-update) | async-done | bytes 12582928 | tf_op jit(solution)/shard_map/all_gather | solution.py:49
  1891.3 44.7 %all-gather.26.cloned.1.call-done = f32[3,256,2048]{2,1,0:T(8,128)} async-done(((f32[3,256,512]{2,1,0:T(8,128)}), f32[3,256,2048]{2,1,0:T(8,128)}) %all-gather.26.cloned.1.call-update) | async-done | bytes 6291472 | tf_op jit(solution)/shard_map/all_gather | solution.py:52
  1936.0 26.9 convolution_add_fusion.1
  1986.6 436.4 %all-gather.38.cloned.1.call-done = f32[2048,512]{1,0:T(8,128)} async-done(((f32[256,512]{1,0:T(8,128)}), f32[2048,512]{1,0:T(8,128)}) %all-gather.38.cloned.1.call-update) | async-done | bytes 4194320 | tf_op jit(solution)/shard_map/all_gather | solution.py:38
  2430.3 97.8 %all-to-all-done.2 = f32[8,2,256,1408]{3,2,1,0:T(8,128)} async-done(((f32[8,2,256,1408]{3,2,1,0:T(8,128)}), f32[8,2,256,1408]{3,2,1,0:T(8,128)}, u32[]{:S(2)}, u32[]{:S(2)}) %all-to-all-start.2) | async-done | bytes 23068704 | tf_op jit(solution)/shard_map/all_to_all | solution.py:36
  2536.9 24.4 fusion.10
  2566.2 56.1 %reduce-scatter.8.cloned.1.call-done = f32[3,256,512]{2,1,0:T(8,128)} async-done(((f32[3,256,2048]{2,1,0:T(8,128)}), f32[3,256,512]{2,1,0:T(8,128)}) %reduce-scatter.8.cloned.1.call-update) | async-done | bytes 1572880 | tf_op jit(solution)/shard_map/reduce_scatter | solution.py:46
  2622.9 47.3 %all-gather.28.cloned.1.call-done = f32[3,256,2048]{2,1,0:T(8,128)} async-done(((f32[3,256,512]{2,1,0:T(8,128)}), f32[3,256,2048]{2,1,0:T(8,128)}) %all-gather.28.cloned.1.call-update) | async-done | bytes 6291472 | tf_op jit(solution)/shard_map/all_gather | solution.py:47
  2670.2 178.2 %all-gather.30.cloned.1.call-done = f32[3,2048,512]{2,1,0:T(8,128)} async-done(((f32[3,256,512]{2,1,0:T(8,128)}), f32[3,2048,512]{2,1,0:T(8,128)}) %all-gather.30.cloned.1.call-update) | async-done | bytes 12582928 | tf_op jit(solution)/shard_map/all_gather | solution.py:49
  2866.1 44.7 %all-gather.32.cloned.1.call-done = f32[3,256,2048]{2,1,0:T(8,128)} async-done(((f32[3,256,512]{2,1,0:T(8,128)}), f32[3,256,2048]{2,1,0:T(8,128)}) %all-gather.32.cloned.1.call-update) | async-done | bytes 6291472 | tf_op jit(solution)/shard_map/all_gather | solution.py:52
  2910.8 46.1 %broadcast_multiply_fusion = (f32[2,256,1408]{2,1,0:T(8,128)}, f32[2,256,1408]{2,1,0:T(8,128)}) fusion(f32[2,256,1408]{2,1,0:T(8,128)} %param.6, f32[3,256,2048]{2,1,0:T(8,128)} %all-gather.32.cloned.1.call-done, f32[2,2048,1408]{2,1,0:T(8,128)} %bitcast.64, f32[2,256,1408]{2,1,0:T(8,128)S(1)} %copy-done.5), kind=kOutput, calls=%fused_computation.22 | convolution fusion | flops 17720344576 | bytes 40894464 | tf_op jit(solution)/shard_map/krs,ksc->krc/dot_general | solution.py:54
  (86 shorter events, 205.4 us)
Async XLA Ops:
  10.4 949.6 %copy-start.3 = (f32[2,256,1408]{2,1,0:T(8,128)}, f32[2,256,1408]{2,1,0:T(8,128)S(1)}, u32[]{:S(2)}) copy-start(f32[2,256,1408]{2,1,0:T(8,128)S(1)} %get-tuple-element.9) | copy-start | bytes 8650756
  20.2 556.3 %all-to-all-start = ((f32[8,2,256,1408]{3,2,1,0:T(8,128)}), f32[8,2,256,1408]{3,2,1,0:T(8,128)}, u32[]{:S(2)}, u32[]{:S(2)}) async-start(f32[8,2,256,1408]{3,2,1,0:T(8,128)} %stack.6), calls=%async_computation | async-start | bytes 46137344 | tf_op jit(solution)/shard_map/all_to_all | solution.py:36
  27.7 443.8 %all-gather.34.cloned.1.call-start = ((), (), s32[]{:S(2)}) async-start(), calls=%async_computation.18 | async-start | bytes 4718592 | tf_op jit(solution)/shard_map/all_gather | solution.py:38
  30.3 640.5 %reduce-scatter.4.cloned.1.call-start = ((), (), s32[]{:S(2)}) async-start(), calls=%async_computation.6 | async-start | bytes 7864320 | tf_op jit(solution)/shard_map/reduce_scatter | solution.py:46
  613.7 105.9 %all-gather.16.cloned.1.call-start = ((), (), s32[]{:S(2)}) async-start(), calls=%async_computation.7 | async-start | bytes 7864320 | tf_op jit(solution)/shard_map/all_gather | solution.py:47
  670.8 227.0 %all-gather.18.cloned.1.call-start = ((), (), s32[]{:S(2)}) async-start(), calls=%async_computation.8 | async-start | bytes 14155776 | tf_op jit(solution)/shard_map/all_gather | solution.py:49
  671.3 288.6 %all-gather.20.cloned.1.call-start = ((), (), s32[]{:S(2)}) async-start(), calls=%async_computation.9 | async-start | bytes 7864320 | tf_op jit(solution)/shard_map/all_gather | solution.py:52
  999.4 555.3 %all-to-all-start.1 = ((f32[8,2,256,1408]{3,2,1,0:T(8,128)}), f32[8,2,256,1408]{3,2,1,0:T(8,128)}, u32[]{:S(2)}, u32[]{:S(2)}) async-start(f32[8,2,256,1408]{3,2,1,0:T(8,128)} %stack.7), calls=%async_computation.2 | async-start | bytes 46137344 | tf_op jit(solution)/shard_map/all_to_all | solution.py:36
  1005.8 443.8 %all-gather.36.cloned.1.call-start = ((), (), s32[]{:S(2)}) async-start(), calls=%async_computation.19 | async-start | bytes 4718592 | tf_op jit(solution)/shard_map/all_gather | solution.py:38
  1014.4 634.5 %reduce-scatter.6.cloned.1.call-start = ((), (), s32[]{:S(2)}) async-start(), calls=%async_computation.10 | async-start | bytes 7864320 | tf_op jit(solution)/shard_map/reduce_scatter | solution.py:46
  1592.8 104.1 %all-gather.22.cloned.1.call-start = ((), (), s32[]{:S(2)}) async-start(), calls=%async_computation.11 | async-start | bytes 7864320 | tf_op jit(solution)/shard_map/all_gather | solution.py:47
  1648.9 226.3 %copy-start.7 = (f32[3,256,512]{2,1,0:T(8,128)S(1)}, f32[3,256,512]{2,1,0:T(8,128)}, u32[]{:S(2)}) copy-start(f32[3,256,512]{2,1,0:T(8,128)} %reduce-scatter.6.cloned.1.call-done) | copy-start | bytes 4718596
  1648.9 226.3 %all-gather.24.cloned.1.call-start = ((), (), s32[]{:S(2)}) async-start(), calls=%async_computation.12 | async-start | bytes 14155776 | tf_op jit(solution)/shard_map/all_gather | solution.py:49
  1649.7 286.3 %all-gather.26.cloned.1.call-start = ((), (), s32[]{:S(2)}) async-start(), calls=%async_computation.13 | async-start | bytes 7864320 | tf_op jit(solution)/shard_map/all_gather | solution.py:52
  1972.8 555.3 %all-to-all-start.2 = ((f32[8,2,256,1408]{3,2,1,0:T(8,128)}), f32[8,2,256,1408]{3,2,1,0:T(8,128)}, u32[]{:S(2)}, u32[]{:S(2)}) async-start(f32[8,2,256,1408]{3,2,1,0:T(8,128)} %stack.8), calls=%async_computation.4 | async-start | bytes 46137344 | tf_op jit(solution)/shard_map/all_to_all | solution.py:36
  1979.1 443.8 %all-gather.38.cloned.1.call-start = ((), (), s32[]{:S(2)}) async-start(), calls=%async_computation.20 | async-start | bytes 4718592 | tf_op jit(solution)/shard_map/all_gather | solution.py:38
  1986.5 635.7 %reduce-scatter.8.cloned.1.call-start = ((), (), s32[]{:S(2)}) async-start(), calls=%async_computation.14 | async-start | bytes 7864320 | tf_op jit(solution)/shard_map/reduce_scatter | solution.py:46
  2566.1 104.1 %all-gather.28.cloned.1.call-start = ((), (), s32[]{:S(2)}) async-start(), calls=%async_computation.15 | async-start | bytes 7864320 | tf_op jit(solution)/shard_map/all_gather | solution.py:47
  2622.3 226.1 %all-gather.30.cloned.1.call-start = ((), (), s32[]{:S(2)}) async-start(), calls=%async_computation.16 | async-start | bytes 14155776 | tf_op jit(solution)/shard_map/all_gather | solution.py:49
  2622.9 287.9 %copy-start.5 = (f32[2,256,1408]{2,1,0:T(8,128)S(1)}, f32[2,256,1408]{2,1,0:T(8,128)}, u32[]{:S(2)}) copy-start(f32[2,256,1408]{2,1,0:T(8,128)} %copy-done.4) | copy-start | bytes 8650756
  2622.9 287.9 %all-gather.32.cloned.1.call-start = ((), (), s32[]{:S(2)}) async-start(), calls=%async_computation.17 | async-start | bytes 7864320 | tf_op jit(solution)/shard_map/all_gather | solution.py:52
  2866.1 90.8 %copy-start.8 = (f32[256,512]{1,0:T(8,128)S(1)}, f32[256,512]{1,0:T(8,128)}, u32[]{:S(2)}) copy-start(f32[256,512]{1,0:T(8,128)} %fusion.6) | copy-start | bytes 1572868
  2910.8 46.1 %copy-start.6 = (f32[2048,512]{1,0:T(8,128)S(1)}, f32[2048,512]{1,0:T(8,128)}, u32[]{:S(2)}) copy-start(f32[2048,512]{1,0:T(8,128)} %all-gather.38.cloned.1.call-done) | copy-start | bytes 12582916
  2910.8 46.1 %copy-start.12 = (f32[256,512]{1,0:T(8,128)S(1)}, f32[256,512]{1,0:T(8,128)}, u32[]{:S(2)}) copy-start(f32[256,512]{1,0:T(8,128)} %param.7) | copy-start | bytes 1572868
  (8 other events, 124.7 us)
Sparse Core Ops, SparseCore 0:
  31.2 440.2 all-gather.33
  613.8 56.8 reduce-scatter.3
  672.3 47.2 all-gather.15
  721.6 176.0 all-gather.17
  915.4 44.5 all-gather.19
  1014.5 435.0 all-gather.35
  1592.9 55.9 reduce-scatter.5
  1650.5 46.3 all-gather.21
  1699.1 176.0 all-gather.23
  1891.4 44.5 all-gather.25
  1986.7 436.2 all-gather.37
  2566.3 55.9 reduce-scatter.7
  2623.8 46.3 all-gather.27
  2672.3 176.0 all-gather.29
  2866.3 44.5 all-gather.31
